TPU v7x, 32 devices: a whole 2x2x4 slice. The times are simulated.
32 devices in a mesh: sp: 16 (over z, y, x), tp: 2 (over core).
Axes of the slice: x: 2, y: 2, z: 4, core: 2. Of those that a mesh axis runs over, the one named last changes fastest.
Arguments:
- features: bfloat16 [4096, 1024], P('sp', 'tp'), may hold values from -6 to 6
- lambda_real: float32 [64, 64], P('tp'), may hold values from -4 to 0, as said below
- lambda_imag: float32 [64, 64], P('tp'), may hold values from 0.5 to 201.06177
- log_step: float32 [64], P('tp'), may hold values from -5 to -2
- input_real: float32 [64, 64, 16], P('tp'), may hold values from -2 to 2
- input_imag: float32 [64, 64, 16], P('tp'), may hold values from -2 to 2
- real_output: float32 [64, 16, 64], P('tp'), may hold values from -0.75 to 0.75
- imaginary_output: float32 [64, 16, 64], P('tp'), may hold values from -0.75 to 0.75
- skip_gain: float32 [1024], P('tp'), may hold values from -4 to 4
- value_weight: bfloat16 [1024, 2048], P('tp'), may hold values from -0.1875 to 0.1875
- gate_weight: bfloat16 [1024, 2048], P('tp'), may hold values from -0.1875 to 0.1875
- value_bias: float32 [2048], replicated, may hold values from -3 to 3
- gate_bias: float32 [2048], replicated, may hold values from -3 to 3
Outputs:
- mixed_output: bfloat16 [4096, 2048], P(('sp', 'tp'))
Inputs may be any that keep to these rules, and one draw needn't show every extreme that they name: `lambda_real`: negative.
All inputs are finite; a program needn't handle non-finite values.
Results may differ from a plain program's by a relative error of at most 0.03.
Values may be sent and summed in bfloat16 or wider, within the bound.
A program may use at most 128 MiB of HBM per device.

v0:
```python
import math
import jax
import jax.numpy as jnp
from jax import lax
from jax.sharding import PartitionSpec as P


def prefix(part, axis, combine, identity):
    place = lax.axis_index(axis)
    gathered = jax.tree.map(lambda a: lax.all_gather(a, axis), part)
    state = jax.tree.map(lambda a, e: jnp.zeros_like(a) + jnp.asarray(e, a.dtype), part, identity)

    def one(lap, state):
        return combine(
            state, jax.tree.map(lambda a: lax.dynamic_index_in_dim(a, lap, 0, False), gathered)
        )

    return lax.fori_loop(0, place, one, state)


def discretize(lambda_real, lambda_imag, log_step, input_real, input_imag):
    step_size = jnp.exp(log_step)[:, None]
    magnitude = jnp.exp(lambda_real * step_size)
    phase_arg = lambda_imag * step_size
    trans_re = magnitude * jnp.cos(phase_arg)
    trans_im = magnitude * jnp.sin(phase_arg)
    denominator = lambda_real * lambda_real + lambda_imag * lambda_imag
    num_re = trans_re - 1.0
    f_re = (num_re * lambda_real + trans_im * lambda_imag) / denominator
    f_im = (trans_im * lambda_real - num_re * lambda_imag) / denominator
    bar_re = f_re[..., None] * input_real - f_im[..., None] * input_imag
    bar_im = f_re[..., None] * input_imag + f_im[..., None] * input_real
    return (step_size, bar_re, bar_im)


def powers_flat(lambda_real, lambda_imag, step_size, first, count):
    exponent = (jnp.arange(count, dtype=jnp.int32) + first).astype(jnp.float32)[:, None]
    rate_re = (lambda_real * step_size).reshape(1, -1)
    rate_im = (lambda_imag * step_size).reshape(1, -1)
    magnitude = jnp.exp(exponent * rate_re)
    phase_arg = exponent * rate_im
    return (magnitude * jnp.cos(phase_arg), magnitude * jnp.sin(phase_arg))


def combine(earlier, later):
    a1r, a1i, b1r, b1i = earlier
    a2r, a2i, b2r, b2i = later
    return (
        a1r * a2r - a1i * a2i,
        a1r * a2i + a1i * a2r,
        a2r * b1r - a2i * b1i + b2r,
        a2r * b1i + a2i * b1r + b2i,
    )


def within_blocks(step_re, step_im, bu_re, bu_im, span):
    blocks_re = bu_re.reshape(-1, span, bu_re.shape[1])
    blocks_im = bu_im.reshape(-1, span, bu_im.shape[1])
    h_re = jnp.zeros_like(blocks_re[:, 0])
    h_im = jnp.zeros_like(blocks_im[:, 0])
    rows_re = []
    rows_im = []
    for offset in range(span):
        new_re = step_re * h_re - step_im * h_im + blocks_re[:, offset]
        new_im = step_re * h_im + step_im * h_re + blocks_im[:, offset]
        h_re, h_im = (new_re, new_im)
        rows_re.append(h_re)
        rows_im.append(h_im)
    return (jnp.stack(rows_re, axis=1), jnp.stack(rows_im, axis=1))


def block_carries(span_re, span_im, ends_re, ends_im, start_re, start_im):

    def advance(carried, ends):
        c_re, c_im = carried
        e_re, e_im = ends
        next_re = span_re * c_re - span_im * c_im + e_re
        next_im = span_re * c_im + span_im * c_re + e_im
        return ((next_re, next_im), (c_re, c_im))

    final, entering = lax.scan(advance, (start_re, start_im), (ends_re, ends_im))
    return (final, entering)


def local(
    features,
    lambda_real,
    lambda_imag,
    log_step,
    input_real,
    input_imag,
    real_output,
    imaginary_output,
    skip_gain,
    value_weight,
    gate_weight,
    value_bias,
    gate_bias,
):
    upper_limit = lax.Precision.HIGHEST
    positions = features.shape[0]
    groups = lambda_real.shape[0]
    state_width = lambda_real.shape[1]
    group_size = input_real.shape[2]
    flat_width = groups * state_width
    span = math.gcd(positions, 16)
    step_size, bar_re, bar_im = discretize(
        lambda_real, lambda_imag, log_step, input_real, input_imag
    )
    inner_re, inner_im = powers_flat(lambda_real, lambda_imag, step_size, 1, span)
    whole_re, whole_im = powers_flat(lambda_real, lambda_imag, step_size, positions, 1)
    step_re, step_im = (inner_re[0], inner_im[0])
    span_re, span_im = (inner_re[-1], inner_im[-1])
    widened = features.astype(jnp.float32)
    grouped = widened.reshape(positions, groups, group_size)
    bu_re = jnp.einsum("sgc,gpc->sgp", grouped, bar_re, precision=upper_limit).reshape(
        positions, flat_width
    )
    bu_im = jnp.einsum("sgc,gpc->sgp", grouped, bar_im, precision=upper_limit).reshape(
        positions, flat_width
    )
    local_re, local_im = within_blocks(step_re, step_im, bu_re, bu_im, span)
    ends_re, ends_im = (local_re[:, -1], local_im[:, -1])
    zero_state = jnp.zeros((flat_width,), jnp.float32)
    ones_state = jnp.ones((flat_width,), jnp.float32)
    identity = (ones_state, zero_state, zero_state, zero_state)
    final, entering = block_carries(span_re, span_im, ends_re, ends_im, zero_state, zero_state)
    enter_re = entering[0][:, None]
    enter_im = entering[1][:, None]
    signal_real = local_re + inner_re * enter_re - inner_im * enter_im
    signal_imaginary = local_im + inner_re * enter_im + inner_im * enter_re
    signal_real = signal_real.reshape(positions, flat_width)
    signal_imaginary = signal_imaginary.reshape(positions, flat_width)
    incoming = prefix((whole_re[0], whole_im[0], final[0], final[1]), "sp", combine, identity)
    h_re, h_im = (incoming[2], incoming[3])
    all_re, all_im = powers_flat(lambda_real, lambda_imag, step_size, 1, positions)
    signal_real = signal_real + all_re * h_re - all_im * h_im
    signal_imaginary = signal_imaginary + all_re * h_im + all_im * h_re
    signal_real = signal_real.reshape(positions, groups, state_width)
    signal_imaginary = signal_imaginary.reshape(positions, groups, state_width)
    mixer_response = jnp.einsum(
        "qej,eoj->qeo", signal_real, real_output, precision=upper_limit
    ) - jnp.einsum("qej,eoj->qeo", signal_imaginary, imaginary_output, precision=upper_limit)
    mixer_response = mixer_response.reshape(positions, groups * group_size) + skip_gain * widened
    activated = jax.nn.gelu(mixer_response).astype(jnp.bfloat16)
    model_width = value_weight.shape[1]
    moved = lax.all_to_all(activated, "tp", split_axis=0, concat_axis=1, tiled=True)
    full_value, full_gate = (
        lax.all_gather(value_weight, "tp", axis=0, tiled=True),
        lax.all_gather(gate_weight, "tp", axis=0, tiled=True),
    )
    pieces = lax.axis_size("tp")
    row_total = moved.shape[0]
    slice_width = value_weight.shape[0]
    blocks_act = moved.reshape(row_total, pieces, slice_width)

    def halves(weight):
        partial_value = jnp.einsum(
            "rnc,ncd->nrd",
            blocks_act,
            weight.reshape(pieces, slice_width, model_width),
            preferred_element_type=jnp.float32,
        )
        rounded = lax.optimization_barrier(partial_value.astype(jnp.bfloat16))
        return jnp.sum(rounded.astype(jnp.float32), axis=0)

    value_sum = halves(full_value)
    gate_sum = halves(full_gate)
    value_sum = value_sum + value_bias
    gate_sum = gate_sum + gate_bias
    return (value_sum * jax.nn.sigmoid(gate_sum)).astype(jnp.bfloat16)


def solution(mesh):
    in_specs = (
        P("sp", "tp"),
        P("tp", None),
        P("tp", None),
        P("tp"),
        P("tp", None, None),
        P("tp", None, None),
        P("tp", None, None),
        P("tp", None, None),
        P("tp"),
        P("tp", None),
        P("tp", None),
        P(),
        P(),
    )
    out_specs = P(("sp", "tp"), None)
    return jax.shard_map(local, mesh=mesh, in_specs=in_specs, out_specs=out_specs, check_vma=False)
```

profile of v0, /device:TPU:31, one launch (start us, length us, event | category | flops | bytes accessed | tf_op | source)
XLA Modules:
  0.0 345.9 jit_solution(2314690990529979079)
XLA Ops:
  9.6 2.4 convolution_bitcast_fusion.1
  14.4 6.1 %copy.90 = f32[256,32,64]{2,1,0:T(8,128)} copy(f32[256,32,64]{0,2,1:T(8,128)} %convolution_bitcast_fusion.1) | data formatting | bytes 4194304 | tf_op jit(solution)/shard_map/sgc,gpc->sgp/transpose | solution.py:116
  20.4 5.1 %reshape_reshape.6 = f32[16,16,2048]{2,1,0:T(8,128)} reshape(f32[256,32,64]{2,1,0:T(8,128)} %copy.90) | data formatting | bytes 4194304 | tf_op jit(solution)/shard_map/reshape;reshape | solution.py:57
  25.5 9.8 %fusion.35 = (f32[16,1,2048]{2,1,0:T(1,128)}, f32[16,1,2048]{2,1,0:T(1,128)S(1)}, f32[16,1,2048]{2,1,0:T(1,128)}, f32[16,1,2048]{2,1,0:T(1,128)}, f32[16,1,2048]...) fusion(f32[16,16,2048]{2,1,0:T(8,128)} %reshape_reshape.6), kind=kLoop, calls=%fused_computation.170 | loop fusion | bytes 4194304 | tf_op jit(solution)/shard_map/slice | solution.py:64
  35.3 4.5 %copy.92 = f32[256,32,64]{2,1,0:T(8,128)} copy(f32[256,32,64]{0,2,1:T(8,128)S(1)} %convolution_bitcast_fusion) | data formatting | bytes 4194304 | tf_op jit(solution)/shard_map/sgc,gpc->sgp/transpose | solution.py:119
  39.8 3.6 %reshape_reshape.7 = f32[16,16,2048]{2,1,0:T(8,128)S(1)} reshape(f32[256,32,64]{2,1,0:T(8,128)} %copy.92) | data formatting | bytes 4194304 | tf_op jit(solution)/shard_map/reshape;reshape | solution.py:58
  43.5 1.6 fusion.34
  48.9 48.8 %while.33 = (s32[]{:T(128)}, f32[2048]{0:T(1024)S(1)}, f32[2048]{0:T(1024)S(1)}, f32[16,2048]{1,0:T(8,128)}, f32[16,2048]{1,0:T(8,128)}, /*index=5*/f32[2048]{0:...) while((s32[]{:T(128)}, f32[2048]{0:T(1024)S(1)}, ...), condition=%wide.region_1.2_spmd.clone, body=%wide.region_0.1_spmd.clone.sunk | while | flops 20483 | bytes 180355 | solution.py:81
  97.7 29.1 %all-gather = f32[32768]{0:T(1024)S(1)} all-gather(f32[2048]{0:T(1024)S(1)} %get-tuple-element.127), channel_id=2, replica_groups=mesh['sp'=16,'tp'=2] {'sp'}, dimensions={0}, use_global_device_ids=true | all-gather | bytes 139264 | tf_op jit(solution)/shard_map/all_gather | solution.py:10
  126.9 31.3 %all-gather.1 = f32[32768]{0:T(1024)S(1)} all-gather(f32[2048]{0:T(1024)S(1)} %get-tuple-element.128), channel_id=3, replica_groups=mesh['sp'=16,'tp'=2] {'sp'}, dimensions={0}, use_global_device_ids=true | all-gather | bytes 139264 | tf_op jit(solution)/shard_map/all_gather | solution.py:10
  158.3 29.5 %all-gather.3 = f32[16,1,2048]{2,1,0:T(1,128)S(1)} all-gather(f32[1,1,2048]{2,1,0:T(1,128)S(1)} %reshape.5975), channel_id=1, replica_groups=mesh['sp'=16,'tp'=2] {'sp'}, dimensions={0}, use_global_device_ids=true | all-gather | bytes 139264 | tf_op jit(solution)/shard_map/all_gather | solution.py:10
  188.6 30.9 %all-gather.2 = f32[16,1,2048]{2,1,0:T(1,128)S(1)} all-gather(f32[1,1,2048]{2,1,0:T(1,128)S(1)} %reshape.5973), channel_id=1, replica_groups=mesh['sp'=16,'tp'=2] {'sp'}, dimensions={0}, use_global_device_ids=true | all-gather | bytes 139264 | tf_op jit(solution)/shard_map/all_gather | solution.py:10
  220.2 14.7 %while.32 = (s32[]{:T(128)}, f32[2048]{0:T(1024)S(1)}, f32[2048]{0:T(1024)S(1)}, s32[]{:T(128)}, f32[16,2048]{1,0:T(8,128)}, /*index=5*/f32[16,2048]{1,0:T(8,128...) while((s32[]{:T(128)}, f32[2048]{0:T(1024)S(1)}, ...), condition=%wide.region_3.4_spmd, body=%wide.region_2.3_spmd.sunk | while | flops 16389 | bytes 131223 | solution.py:18
  249.0 2.8 multiply_subtract_fusion.1
  251.9 2.5 copy.126
  254.4 4.9 %add.1212 = f32[256,32,64]{2,1,0:T(8,128)} reshape(f32[16,16,2048]{2,1,0:T(8,128)} %copy.126) | data formatting | bytes 4194304 | tf_op jit(solution)/shard_map/add | solution.py:131
  259.3 2.5 copy.124
  261.8 4.9 %sub.375 = f32[256,32,64]{2,1,0:T(8,128)} reshape(f32[16,16,2048]{2,1,0:T(8,128)} %copy.124) | data formatting | bytes 4194304 | tf_op jit(solution)/shard_map/sub | solution.py:130
  266.7 19.2 %multiply_subtract_fusion = (f32[256,32,64]{2,1,0:T(8,128)S(1)}, f32[256,32,64]{2,1,0:T(8,128)S(1)}) fusion(f32[256,32,64]{2,1,0:T(8,128)} %sub.375, f32[32,64]{1,0:T(8,128)S(1)} %mul.2004, f32[32,64]{1,0:T(8,128)S(1)} %mul.2000, f32[32,64]{1,0:T(8,128)S(1)} %copy-done.52, f32[32,64]{1,0:T(8,128)S(1)} %copy-done.54, f32[256]{0:T(256)S(1)} %add_convert_fusion, ...), kind=kLoop, calls=%fused_computation.21 | loop fusion | flops 6291456 | bytes 8422400 | tf_op jit(solution)/shard_map/sub | solution.py:137
  285.9 6.1 %fusion.2 = f32[32,256,16]{1,2,0:T(8,128)S(1)} fusion(f32[32,16,64]{2,1,0:T(8,128)S(1)} %copy-done, f32[256,32,64]{2,1,0:T(8,128)S(1)} %get-tuple-element.313), kind=kOutput, calls=%fused_computation.16 | convolution fusion | flops 100663296 | bytes 2752512 | tf_op jit(solution)/shard_map/qej,eoj->qeo/dot_general | solution.py:143
  292.1 6.1 %fusion.6 = f32[32,256,16]{1,2,0:T(8,128)S(1)} fusion(f32[32,256,16]{1,2,0:T(8,128)S(1)} %fusion.2, f32[32,16,64]{2,1,0:T(8,128)S(1)} %copy-done.50, f32[256,32,64]{2,1,0:T(8,128)S(1)} %get-tuple-element.312), kind=kOutput, calls=%fused_computation.31 | convolution fusion | flops 100794368 | bytes 3276800 | tf_op jit(solution)/shard_map/qej,eoj->qeo/dot_general | solution.py:141
  298.6 32.4 %all_to_all.16 = bf16[2,128,512]{2,1,0:T(8,128)(2,1)S(1)} all-to-all(bf16[2,128,512]{2,1,0:T(8,128)(2,1)S(1)} %bitcast.277), channel_id=1, replica_groups=mesh['sp'=16,'tp'=2] {'tp'}, dimensions={0} | all-to-all | bytes 524288 | tf_op jit(solution)/shard_map/all_to_all | solution.py:147
  331.0 2.9 convolution_convert_fusion.1
  334.1 2.9 convolution_convert_fusion
  (320 shorter events, 89.2 us)
Async XLA Ops:
  6.5 279.4 %copy-start = (f32[32,16,64]{2,1,0:T(8,128)S(1)}, f32[32,16,64]{2,1,0:T(8,128)}, u32[]{:S(2)}) copy-start(f32[32,16,64]{2,1,0:T(8,128)} %param.24) | copy-start | bytes 393220
  6.6 324.4 %all-gather.7.cloned.1.call-start = ((), (), s32[]{:S(2)}) async-start(), calls=%async_computation.1 | async-start | bytes 6291456 | tf_op jit(solution)/shard_map/all_gather | solution.py:149
  7.3 326.8 %all-gather.9.cloned.1.call-start = ((), (), s32[]{:S(2)}) async-start(), calls=%async_computation.2 | async-start | bytes 6291456 | tf_op jit(solution)/shard_map/all_gather | solution.py:150
  9.6 3.4 copy-start.53
  9.6 4.1 %copy-start.51 = (f32[32,64]{1,0:T(8,128)}, f32[32,64]{1,0:T(8,128)S(1)}, u32[]{:S(2)}) copy-start(f32[32,64]{1,0:T(8,128)S(1)} %get-tuple-element.318) | copy-start | bytes 24580
  43.5 3.5 %copy-start.15 = (f32[16,1,2048]{2,1,0:T(1,128)S(1)}, f32[16,1,2048]{2,1,0:T(1,128)}, u32[]{:S(2)}) copy-start(f32[16,1,2048]{2,1,0:T(1,128)} %get-tuple-element.281) | copy-start | bytes 393220
  43.5 3.5 %copy-start.19 = (f32[16,1,2048]{2,1,0:T(1,128)S(1)}, f32[16,1,2048]{2,1,0:T(1,128)}, u32[]{:S(2)}) copy-start(f32[16,1,2048]{2,1,0:T(1,128)} %get-tuple-element.283) | copy-start | bytes 393220
  43.5 3.5 %copy-start.23 = (f32[16,1,2048]{2,1,0:T(1,128)S(1)}, f32[16,1,2048]{2,1,0:T(1,128)}, u32[]{:S(2)}) copy-start(f32[16,1,2048]{2,1,0:T(1,128)} %get-tuple-element.284) | copy-start | bytes 393220
  48.1 110.1 %copy-start.58 = (f32[32,64]{1,0:T(8,128)S(1)}, f32[32,64]{1,0:T(8,128)}, u32[]{:S(2)}) copy-start(f32[32,64]{1,0:T(8,128)} %get-tuple-element.314) | copy-start | bytes 24580
  48.7 139.8 %copy-start.57 = (f32[32,64]{1,0:T(8,128)S(1)}, f32[32,64]{1,0:T(8,128)}, u32[]{:S(2)}) copy-start(f32[32,64]{1,0:T(8,128)} %get-tuple-element.315) | copy-start | bytes 24580
  48.9 186.0 %copy-start.41 = (f32[16,1,2048]{2,1,0:T(1,128)S(1)}, f32[16,1,2048]{2,1,0:T(1,128)}, u32[]{:S(2)}) copy-start(f32[16,1,2048]{2,1,0:T(1,128)} %get-tuple-element.287) | copy-start | bytes 393220
  48.9 186.8 %copy-start.35 = (f32[16,1,2048]{2,1,0:T(1,128)S(1)}, f32[16,1,2048]{2,1,0:T(1,128)}, u32[]{:S(2)}) copy-start(f32[16,1,2048]{2,1,0:T(1,128)} %get-tuple-element.286) | copy-start | bytes 393220
  48.9 186.8 %copy-start.39 = (f32[16,1,2048]{2,1,0:T(1,128)S(1)}, f32[16,1,2048]{2,1,0:T(1,128)}, u32[]{:S(2)}) copy-start(f32[16,1,2048]{2,1,0:T(1,128)} %copy-done.38) | copy-start | bytes 393220
  126.9 109.8 %copy-start.31 = (f32[16,1,2048]{2,1,0:T(1,128)S(1)}, f32[16,1,2048]{2,1,0:T(1,128)}, u32[]{:S(2)}) copy-start(f32[16,1,2048]{2,1,0:T(1,128)} %get-tuple-element.285) | copy-start | bytes 393220
  126.9 109.8 %copy-start.37 = (f32[16,1,2048]{2,1,0:T(1,128)S(1)}, f32[16,1,2048]{2,1,0:T(1,128)}, u32[]{:S(2)}) copy-start(f32[16,1,2048]{2,1,0:T(1,128)} %copy-done.36) | copy-start | bytes 393220
  220.2 17.3 %copy-start.24 = (f32[16,1,2048]{2,1,0:T(1,128)S(1)}, f32[16,1,2048]{2,1,0:T(1,128)}, u32[]{:S(2)}) copy-start(f32[16,1,2048]{2,1,0:T(1,128)} %get-tuple-element.284) | copy-start | bytes 393220
  220.2 17.3 %copy-start.33 = (f32[16,1,2048]{2,1,0:T(1,128)S(1)}, f32[16,1,2048]{2,1,0:T(1,128)}, u32[]{:S(2)}) copy-start(f32[16,1,2048]{2,1,0:T(1,128)} %copy-done.32) | copy-start | bytes 393220
  245.0 4.0 %copy-start.47 = (f32[16,2048]{1,0:T(8,128)S(1)}, f32[16,2048]{1,0:T(8,128)}, u32[]{:S(2)}) copy-start(f32[16,2048]{1,0:T(8,128)} %copy-done.46) | copy-start | bytes 393220
  245.0 4.0 %copy-start.49 = (f32[16,2048]{1,0:T(8,128)S(1)}, f32[16,2048]{1,0:T(8,128)}, u32[]{:S(2)}) copy-start(f32[16,2048]{1,0:T(8,128)} %copy-done.48) | copy-start | bytes 393220
  261.8 4.9 %copy-start.52 = (f32[32,64]{1,0:T(8,128)S(1)}, f32[32,64]{1,0:T(8,128)}, u32[]{:S(2)}) copy-start(f32[32,64]{1,0:T(8,128)} %copy-done.51) | copy-start | bytes 24580
  261.8 4.9 %copy-start.54 = (f32[32,64]{1,0:T(8,128)S(1)}, f32[32,64]{1,0:T(8,128)}, u32[]{:S(2)}) copy-start(f32[32,64]{1,0:T(8,128)} %copy-done.53) | copy-start | bytes 24580
  285.9 6.1 %copy-start.50 = (f32[32,16,64]{2,1,0:T(8,128)S(1)}, f32[32,16,64]{2,1,0:T(8,128)}, u32[]{:S(2)}) copy-start(f32[32,16,64]{2,1,0:T(8,128)} %param.23) | copy-start | bytes 393220
  292.0 6.3 %copy-start.45 = (bf16[256,512]{1,0:T(8,128)(2,1)S(1)}, bf16[256,512]{1,0:T(8,128)(2,1)}, u32[]{:S(2)}) copy-start(bf16[256,512]{1,0:T(8,128)(2,1)} %param.17) | copy-start | bytes 786436
  292.0 6.3 %copy-start.65 = (f32[512]{0:T(512)S(1)}, f32[512]{0:T(512)}, u32[]{:S(2)}) copy-start(f32[512]{0:T(512)} %param.25) | copy-start | bytes 6148
  (46 other events, 112.8 us)
Sparse Core Ops, SparseCore 0:
  8.9 15.2 all-gather.6
  25.8 14.8 all-gather.8
where the time goes:
time: 351 us; the launch traced here: 346 us
  blocking collectives  153 us (44%)
  local copies, waits for them, and re-layouts  112 us (32%)
  other arithmetic  41.9 us (12%)
  matrix products  21.4 us (6%)
  between operations  14.5 us (4%)
    all_gather x4, blocking collectives, prefix(): gathered = jax.tree.map(lambda a: lax.all_gather(a, axis), part)  121 us
    dynamic_update_slice x32, local copies, waits for them, and re-layouts, block_carries(): lax.scan(advance, (start_re, start_im), (ends_re, ends_im))  47.9 us
    all_to_all x1, blocking collectives, local(): lax.all_to_all(activated, 'tp', split_axis=0, concat_axis=1, tiled=True)  32.4 us
    sub x1, other arithmetic, local(): signal_real = signal_real + all_re * h_re - all_im * h_im  19.2 us
    dynamic_slice x30, local copies, waits for them, and re-layouts, one(): lax.dynamic_index_in_dim(a, lap, 0, False)  13.7 us
    unnamed x17, other arithmetic  12.3 us
    slice x1, local copies, waits for them, and re-layouts, within_blocks(): new_re = step_re * h_re - step_im * h_im + blocks_re[:, offset]  9.78 us
    sub x2, local copies, waits for them, and re-layouts, local(): signal_real = local_re + inner_re * enter_re - inner_im * enter_im  7.42 us
  transfers between devices with their start and end apart: 2, of which 0 were waited for; matrix products, arithmetic and copies ran while one was open for 49% of the time, Pallas kernels for 0%

commit v1 on v0

--- a/solution.py
+++ b/solution.py
@@ -144,7 +144,10 @@
     mixer_response = mixer_response.reshape(positions, groups * group_size) + skip_gain * widened
     activated = jax.nn.gelu(mixer_response).astype(jnp.bfloat16)
     model_width = value_weight.shape[1]
-    moved = lax.all_to_all(activated, "tp", split_axis=0, concat_axis=1, tiled=True)
+    moved = jnp.concatenate(
+        lax.all_to_all(jnp.stack(jnp.split(activated, lax.axis_size("tp"), axis=0)), "tp", 0, 0),
+        axis=1,
+    )
     full_value, full_gate = (
         lax.all_gather(value_weight, "tp", axis=0, tiled=True),
         lax.all_gather(gate_weight, "tp", axis=0, tiled=True),

time: 351 us -> 351 us (level)
  no operation moved by 1% of the time
where the time goes in v1:
time: 351 us; the launch traced here: 346 us
  blocking collectives  153 us (44%)
  local copies, waits for them, and re-layouts  112 us (32%)
  other arithmetic  41.9 us (12%)
  matrix products  21.4 us (6%)
  between operations  14.5 us (4%)
    all_gather x4, blocking collectives, prefix(): gathered = jax.tree.map(lambda a: lax.all_gather(a, axis), part)  120 us
    dynamic_update_slice x32, local copies, waits for them, and re-layouts, block_carries(): lax.scan(advance, (start_re, start_im), (ends_re, ends_im))  47.6 us
    all_to_all x1, blocking collectives, local(): lax.all_to_all(jnp.stack(jnp.split(activated, lax.axis_size('tp'), axis=0...  32.7 us
    sub x1, other arithmetic, local(): signal_real = signal_real + all_re * h_re - all_im * h_im  19.2 us
    dynamic_slice x30, local copies, waits for them, and re-layouts, one(): lax.dynamic_index_in_dim(a, lap, 0, False)  13.7 us
    unnamed x17, other arithmetic  12.3 us
    slice x1, local copies, waits for them, and re-layouts, within_blocks(): new_re = step_re * h_re - step_im * h_im + blocks_re[:, offset]  9.73 us
    sub x2, local copies, waits for them, and re-layouts, local(): signal_real = local_re + inner_re * enter_re - inner_im * enter_im  7.41 us
  transfers between devices with their start and end apart: 2, of which 0 were waited for; matrix products, arithmetic and copies ran while one was open for 49% of the time, Pallas kernels for 0%

profile of v1, /device:TPU:31, one launch (start us, length us, event | category | flops | bytes accessed | tf_op | source)
XLA Modules:
  0.0 345.6 jit_solution(6687949648943361616)
XLA Ops:
  9.6 2.3 convolution_bitcast_fusion.1
  14.4 6.0 %copy.90 = f32[256,32,64]{2,1,0:T(8,128)} copy(f32[256,32,64]{0,2,1:T(8,128)} %convolution_bitcast_fusion.1) | data formatting | bytes 4194304 | tf_op jit(solution)/shard_map/sgc,gpc->sgp/transpose | solution.py:116
  20.5 5.2 %reshape_reshape.6 = f32[16,16,2048]{2,1,0:T(8,128)} reshape(f32[256,32,64]{2,1,0:T(8,128)} %copy.90) | data formatting | bytes 4194304 | tf_op jit(solution)/shard_map/reshape;reshape | solution.py:57
  25.7 9.7 %fusion.35 = (f32[16,1,2048]{2,1,0:T(1,128)}, f32[16,1,2048]{2,1,0:T(1,128)S(1)}, f32[16,1,2048]{2,1,0:T(1,128)}, f32[16,1,2048]{2,1,0:T(1,128)}, f32[16,1,2048]...) fusion(f32[16,16,2048]{2,1,0:T(8,128)} %reshape_reshape.6), kind=kLoop, calls=%fused_computation.173 | loop fusion | bytes 4194304 | tf_op jit(solution)/shard_map/slice | solution.py:64
  35.4 4.5 %copy.92 = f32[256,32,64]{2,1,0:T(8,128)} copy(f32[256,32,64]{0,2,1:T(8,128)S(1)} %convolution_bitcast_fusion) | data formatting | bytes 4194304 | tf_op jit(solution)/shard_map/sgc,gpc->sgp/transpose | solution.py:119
  39.9 3.6 %reshape_reshape.7 = f32[16,16,2048]{2,1,0:T(8,128)S(1)} reshape(f32[256,32,64]{2,1,0:T(8,128)} %copy.92) | data formatting | bytes 4194304 | tf_op jit(solution)/shard_map/reshape;reshape | solution.py:58
  43.6 1.6 fusion.34
  49.0 48.5 %while.33 = (s32[]{:T(128)}, f32[2048]{0:T(1024)S(1)}, f32[2048]{0:T(1024)S(1)}, f32[16,2048]{1,0:T(8,128)}, f32[16,2048]{1,0:T(8,128)}, /*index=5*/f32[2048]{0:...) while((s32[]{:T(128)}, f32[2048]{0:T(1024)S(1)}, ...), condition=%wide.region_1.2_spmd.clone, body=%wide.region_0.1_spmd.clone.sunk | while | flops 20483 | bytes 180355 | solution.py:81
  97.6 28.9 %all-gather = f32[32768]{0:T(1024)S(1)} all-gather(f32[2048]{0:T(1024)S(1)} %get-tuple-element.127), channel_id=2, replica_groups=mesh['sp'=16,'tp'=2] {'sp'}, dimensions={0}, use_global_device_ids=true | all-gather | bytes 139264 | tf_op jit(solution)/shard_map/all_gather | solution.py:10
  126.6 31.3 %all-gather.1 = f32[32768]{0:T(1024)S(1)} all-gather(f32[2048]{0:T(1024)S(1)} %get-tuple-element.128), channel_id=3, replica_groups=mesh['sp'=16,'tp'=2] {'sp'}, dimensions={0}, use_global_device_ids=true | all-gather | bytes 139264 | tf_op jit(solution)/shard_map/all_gather | solution.py:10
  158.0 29.2 %all-gather.3 = f32[16,1,2048]{2,1,0:T(1,128)S(1)} all-gather(f32[1,1,2048]{2,1,0:T(1,128)S(1)} %reshape.5974), channel_id=1, replica_groups=mesh['sp'=16,'tp'=2] {'sp'}, dimensions={0}, use_global_device_ids=true | all-gather | bytes 139264 | tf_op jit(solution)/shard_map/all_gather | solution.py:10
  188.0 30.9 %all-gather.2 = f32[16,1,2048]{2,1,0:T(1,128)S(1)} all-gather(f32[1,1,2048]{2,1,0:T(1,128)S(1)} %reshape.5972), channel_id=1, replica_groups=mesh['sp'=16,'tp'=2] {'sp'}, dimensions={0}, use_global_device_ids=true | all-gather | bytes 139264 | tf_op jit(solution)/shard_map/all_gather | solution.py:10
  219.6 14.7 %while.32 = (s32[]{:T(128)}, f32[2048]{0:T(1024)S(1)}, f32[2048]{0:T(1024)S(1)}, s32[]{:T(128)}, f32[16,2048]{1,0:T(8,128)}, /*index=5*/f32[16,2048]{1,0:T(8,128...) while((s32[]{:T(128)}, f32[2048]{0:T(1024)S(1)}, ...), condition=%wide.region_3.4_spmd, body=%wide.region_2.3_spmd.sunk | while | flops 16389 | bytes 131223 | solution.py:18
  248.3 2.8 multiply_subtract_fusion.1
  251.2 2.5 copy.126
  253.7 4.9 %add.1212 = f32[256,32,64]{2,1,0:T(8,128)} reshape(f32[16,16,2048]{2,1,0:T(8,128)} %copy.126) | data formatting | bytes 4194304 | tf_op jit(solution)/shard_map/add | solution.py:131
  258.6 2.5 copy.124
  261.1 4.9 %sub.375 = f32[256,32,64]{2,1,0:T(8,128)} reshape(f32[16,16,2048]{2,1,0:T(8,128)} %copy.124) | data formatting | bytes 4194304 | tf_op jit(solution)/shard_map/sub | solution.py:130
  266.0 19.2 %multiply_subtract_fusion = (f32[256,32,64]{2,1,0:T(8,128)S(1)}, f32[256,32,64]{2,1,0:T(8,128)S(1)}) fusion(f32[256,32,64]{2,1,0:T(8,128)} %sub.375, f32[32,64]{1,0:T(8,128)S(1)} %mul.2004, f32[32,64]{1,0:T(8,128)S(1)} %mul.2000, f32[32,64]{1,0:T(8,128)S(1)} %copy-done.52, f32[32,64]{1,0:T(8,128)S(1)} %copy-done.54, f32[256]{0:T(256)S(1)} %add_convert_fusion, ...), kind=kLoop, calls=%fused_computation.21 | loop fusion | flops 6291456 | bytes 8422400 | tf_op jit(solution)/shard_map/sub | solution.py:137
  285.2 6.1 %fusion.2 = f32[32,256,16]{1,2,0:T(8,128)S(1)} fusion(f32[32,16,64]{2,1,0:T(8,128)S(1)} %copy-done, f32[256,32,64]{2,1,0:T(8,128)S(1)} %get-tuple-element.315), kind=kOutput, calls=%fused_computation.16 | convolution fusion | flops 100663296 | bytes 2752512 | tf_op jit(solution)/shard_map/qej,eoj->qeo/dot_general | solution.py:143
  291.4 6.1 %fusion.6 = f32[32,256,16]{1,2,0:T(8,128)S(1)} fusion(f32[32,256,16]{1,2,0:T(8,128)S(1)} %fusion.2, f32[32,16,64]{2,1,0:T(8,128)S(1)} %copy-done.50, f32[256,32,64]{2,1,0:T(8,128)S(1)} %get-tuple-element.314), kind=kOutput, calls=%fused_computation.31 | convolution fusion | flops 100794368 | bytes 3276800 | tf_op jit(solution)/shard_map/qej,eoj->qeo/dot_general | solution.py:141
  298.0 32.7 %all_to_all.5 = bf16[2,128,512]{2,1,0:T(8,128)(2,1)S(1)} all-to-all(bf16[2,128,512]{2,1,0:T(8,128)(2,1)S(1)} %pad_maximum_fusion), channel_id=1, replica_groups=mesh['sp'=16,'tp'=2] {'tp'}, dimensions={0} | all-to-all | bytes 524288 | tf_op jit(solution)/shard_map/all_to_all | solution.py:148
  330.7 2.9 convolution_convert_fusion.1
  333.8 2.9 convolution_convert_fusion
  (322 shorter events, 88.9 us)
Async XLA Ops:
  6.5 278.7 %copy-start = (f32[32,16,64]{2,1,0:T(8,128)S(1)}, f32[32,16,64]{2,1,0:T(8,128)}, u32[]{:S(2)}) copy-start(f32[32,16,64]{2,1,0:T(8,128)} %param.24) | copy-start | bytes 393220
  6.6 324.1 %all-gather.7.cloned.1.call-start = ((), (), s32[]{:S(2)}) async-start(), calls=%async_computation.1 | async-start | bytes 6291456 | tf_op jit(solution)/shard_map/all_gather | solution.py:152
  7.3 326.5 %all-gather.9.cloned.1.call-start = ((), (), s32[]{:S(2)}) async-start(), calls=%async_computation.2 | async-start | bytes 6291456 | tf_op jit(solution)/shard_map/all_gather | solution.py:153
  9.6 3.4 copy-start.53
  9.6 4.1 %copy-start.51 = (f32[32,64]{1,0:T(8,128)}, f32[32,64]{1,0:T(8,128)S(1)}, u32[]{:S(2)}) copy-start(f32[32,64]{1,0:T(8,128)S(1)} %get-tuple-element.320) | copy-start | bytes 24580
  43.6 3.5 %copy-start.15 = (f32[16,1,2048]{2,1,0:T(1,128)S(1)}, f32[16,1,2048]{2,1,0:T(1,128)}, u32[]{:S(2)}) copy-start(f32[16,1,2048]{2,1,0:T(1,128)} %get-tuple-element.281) | copy-start | bytes 393220
  43.6 3.5 %copy-start.19 = (f32[16,1,2048]{2,1,0:T(1,128)S(1)}, f32[16,1,2048]{2,1,0:T(1,128)}, u32[]{:S(2)}) copy-start(f32[16,1,2048]{2,1,0:T(1,128)} %get-tuple-element.283) | copy-start | bytes 393220
  43.6 3.5 %copy-start.23 = (f32[16,1,2048]{2,1,0:T(1,128)S(1)}, f32[16,1,2048]{2,1,0:T(1,128)}, u32[]{:S(2)}) copy-start(f32[16,1,2048]{2,1,0:T(1,128)} %get-tuple-element.284) | copy-start | bytes 393220
  48.2 109.7 %copy-start.58 = (f32[32,64]{1,0:T(8,128)S(1)}, f32[32,64]{1,0:T(8,128)}, u32[]{:S(2)}) copy-start(f32[32,64]{1,0:T(8,128)} %get-tuple-element.316) | copy-start | bytes 24580
  48.8 139.1 %copy-start.57 = (f32[32,64]{1,0:T(8,128)S(1)}, f32[32,64]{1,0:T(8,128)}, u32[]{:S(2)}) copy-start(f32[32,64]{1,0:T(8,128)} %get-tuple-element.317) | copy-start | bytes 24580
  49.0 185.3 %copy-start.41 = (f32[16,1,2048]{2,1,0:T(1,128)S(1)}, f32[16,1,2048]{2,1,0:T(1,128)}, u32[]{:S(2)}) copy-start(f32[16,1,2048]{2,1,0:T(1,128)} %get-tuple-element.287) | copy-start | bytes 393220
  49.0 186.1 %copy-start.35 = (f32[16,1,2048]{2,1,0:T(1,128)S(1)}, f32[16,1,2048]{2,1,0:T(1,128)}, u32[]{:S(2)}) copy-start(f32[16,1,2048]{2,1,0:T(1,128)} %get-tuple-element.286) | copy-start | bytes 393220
  49.0 186.1 %copy-start.39 = (f32[16,1,2048]{2,1,0:T(1,128)S(1)}, f32[16,1,2048]{2,1,0:T(1,128)}, u32[]{:S(2)}) copy-start(f32[16,1,2048]{2,1,0:T(1,128)} %copy-done.38) | copy-start | bytes 393220
  126.5 109.5 %copy-start.31 = (f32[16,1,2048]{2,1,0:T(1,128)S(1)}, f32[16,1,2048]{2,1,0:T(1,128)}, u32[]{:S(2)}) copy-start(f32[16,1,2048]{2,1,0:T(1,128)} %get-tuple-element.285) | copy-start | bytes 393220
  126.6 109.5 %copy-start.37 = (f32[16,1,2048]{2,1,0:T(1,128)S(1)}, f32[16,1,2048]{2,1,0:T(1,128)}, u32[]{:S(2)}) copy-start(f32[16,1,2048]{2,1,0:T(1,128)} %copy-done.36) | copy-start | bytes 393220
  219.6 17.3 %copy-start.24 = (f32[16,1,2048]{2,1,0:T(1,128)S(1)}, f32[16,1,2048]{2,1,0:T(1,128)}, u32[]{:S(2)}) copy-start(f32[16,1,2048]{2,1,0:T(1,128)} %get-tuple-element.284) | copy-start | bytes 393220
  219.6 17.3 %copy-start.33 = (f32[16,1,2048]{2,1,0:T(1,128)S(1)}, f32[16,1,2048]{2,1,0:T(1,128)}, u32[]{:S(2)}) copy-start(f32[16,1,2048]{2,1,0:T(1,128)} %copy-done.32) | copy-start | bytes 393220
  244.3 4.0 %copy-start.47 = (f32[16,2048]{1,0:T(8,128)S(1)}, f32[16,2048]{1,0:T(8,128)}, u32[]{:S(2)}) copy-start(f32[16,2048]{1,0:T(8,128)} %copy-done.46) | copy-start | bytes 393220
  244.3 4.0 %copy-start.49 = (f32[16,2048]{1,0:T(8,128)S(1)}, f32[16,2048]{1,0:T(8,128)}, u32[]{:S(2)}) copy-start(f32[16,2048]{1,0:T(8,128)} %copy-done.48) | copy-start | bytes 393220
  261.1 4.9 %copy-start.52 = (f32[32,64]{1,0:T(8,128)S(1)}, f32[32,64]{1,0:T(8,128)}, u32[]{:S(2)}) copy-start(f32[32,64]{1,0:T(8,128)} %copy-done.51) | copy-start | bytes 24580
  261.1 4.9 %copy-start.54 = (f32[32,64]{1,0:T(8,128)S(1)}, f32[32,64]{1,0:T(8,128)}, u32[]{:S(2)}) copy-start(f32[32,64]{1,0:T(8,128)} %copy-done.53) | copy-start | bytes 24580
  285.2 6.1 %copy-start.50 = (f32[32,16,64]{2,1,0:T(8,128)S(1)}, f32[32,16,64]{2,1,0:T(8,128)}, u32[]{:S(2)}) copy-start(f32[32,16,64]{2,1,0:T(8,128)} %param.23) | copy-start | bytes 393220
  291.3 6.3 %copy-start.45 = (bf16[256,512]{1,0:T(8,128)(2,1)S(1)}, bf16[256,512]{1,0:T(8,128)(2,1)}, u32[]{:S(2)}) copy-start(bf16[256,512]{1,0:T(8,128)(2,1)} %param.17) | copy-start | bytes 786436
  291.3 6.3 %copy-start.65 = (f32[512]{0:T(512)S(1)}, f32[512]{0:T(512)}, u32[]{:S(2)}) copy-start(f32[512]{0:T(512)} %param.25) | copy-start | bytes 6148
  (46 other events, 113.1 us)
Sparse Core Ops, SparseCore 0:
  8.9 15.2 all-gather.6
  25.8 14.8 all-gather.8
